TPU v7x, 512 devices: a whole 4x4x16 slice. The times are simulated.
512 devices in a mesh: fs: 16 (over y, x), tp: 32 (over z, core).
Axes of the slice: x: 4, y: 4, z: 16, core: 2. Of those that a mesh axis runs over, the one named last changes fastest.
Arguments:
- tokens: bfloat16 [4096, 2048], P('fs', 'tp'), may hold values from -60 to 60
- norm_gain: float32 [2048], P('fs'), may hold values from 0.1 to 1.9
- gate_weight: float32 [16, 2048, 4096], P(None, 'fs', 'tp'), may hold values from -0.125 to 0.125
- up_weight: float32 [16, 2048, 4096], P(None, 'fs', 'tp'), may hold values from -0.125 to 0.125
- down_weight: float32 [16, 2048, 4096], P(None, 'fs', 'tp'), may hold values from -0.1875 to 0.1875
- route: int32 [4096, 2], P('fs'), may hold values from 0 to 15, all different within a row; in each aligned block of 256 rows (0 to 255, 256 to 511, ...) at most 64 rows name the same one
- route_weight: float32 [4096, 2], P('fs'), may hold values from 0.2 to 1
Outputs:
- mixed: bfloat16 [4096, 2048], P('fs', 'tp')
- gate_new: bfloat16 [16, 2048, 4096], P('fs', None, 'tp')
- up_new: bfloat16 [16, 2048, 4096], P('fs', None, 'tp')
- down_new: bfloat16 [16, 2048, 4096], P('fs', None, 'tp')
Inputs may be any that keep to these rules, and one draw needn't show every extreme that they name: `route`: the 2 experts of a row differ. In each aligned block of 256 rows (the tokens of one index of fs) no expert is named by more than 64 rows, a bound that some block reaches.
All inputs are finite; a program needn't handle non-finite values.
Results may differ from a plain program's by a relative error of at most 0.024.
Values may be sent and summed in bfloat16 or wider, within the bound.
A program may use at most 64 MiB of HBM per device.

v0:
```python
import jax
import jax.numpy as jnp
from jax import lax
from jax.sharding import Mesh
from jax.sharding import PartitionSpec as P

TP = ("tp_0", "tp_1")
epsilon = 1e-05


def sent_together(arrays, axis, split_dim, concat_dim, along):
    both = jnp.concatenate(arrays, axis=along)
    whole, at, done = (
        lax.all_to_all(both, axis, split_axis=split_dim, concat_axis=concat_dim, tiled=True),
        0,
        [],
    )
    for a in arrays:
        done.append(lax.slice_in_dim(whole, at, at + a.shape[along], axis=along))
        at += a.shape[along]
    return tuple(done)


def sent_to_all(x, axis):
    peers = lax.axis_size(axis)
    return lax.all_to_all(jnp.broadcast_to(x[None], (peers, *x.shape)), axis, 0, 0, tiled=True)


def taken_together(x, axis):
    return sent_to_all(x, axis).sum(axis=0)


def reduced_to_own(pieces, axes, turns):
    shape = [lax.axis_size(a) for a in axes]
    pieces = pieces.reshape(*shape, *pieces.shape[1:])
    pieces = pieces.transpose(*turns, *range(len(axes), pieces.ndim))
    pieces = pieces.reshape(-1, *pieces.shape[len(axes) :])
    for k in turns:
        pieces = lax.psum_scatter(pieces, axes[k], scatter_dimension=0, tiled=True)
    return pieces[0]


def in_blocks(x, dim, peers):
    shape = x.shape
    pieces = x.reshape(*shape[:dim], peers, shape[dim] // peers, *shape[dim + 1 :])
    return jnp.moveaxis(pieces, dim, 0)


def scatter_axes(x, axes, turns, dim):
    peers = lax.axis_size(axes)
    return reduced_to_own(in_blocks(x, dim, peers), axes, turns)


def slot_table(route, block_rows, expert_count):
    pair_ids = route.reshape(-1, block_rows * route.shape[1])
    onehot = (
        pair_ids[:, :, None] == jnp.arange(expert_count, dtype=jnp.int32)[None, None, :]
    ).astype(jnp.int32)
    before = jnp.cumsum(onehot, axis=1) - onehot
    return jnp.sum(before * onehot, axis=2).reshape(route.shape)


def body(tokens, norm_gain, gate_weight, up_weight, down_weight, route, route_weight):
    experts = gate_weight.shape[0]
    tok_rows = tokens.shape[0]
    columns = tokens.shape[1]
    fs_count = lax.axis_size("fs")
    capacity = 4 * tok_rows // fs_count
    gain_col = norm_gain[None, :, None]
    gate_cast = (gate_weight * gain_col).astype(jnp.bfloat16)
    up_cast = (up_weight * gain_col).astype(jnp.bfloat16)
    down_cast = down_weight.astype(jnp.bfloat16)
    gate_new, up_new, down_new = sent_together((gate_cast, up_cast, down_cast), "fs", 0, 1, 2)
    slot_of = slot_table(route, tok_rows, experts)
    target = route * capacity + slot_of
    slot_lanes = jnp.arange(experts * capacity, dtype=jnp.int32)
    slot_hits = target[:, :, None] == slot_lanes[None, None, :]
    token_iota = jnp.arange(tok_rows, dtype=jnp.int32)[:, None, None]
    lane_token = jnp.sum(jnp.where(slot_hits, token_iota + 1, 0), axis=(0, 1)) - 1
    lane_token = jnp.where(lane_token < 0, tok_rows, lane_token)
    combine = jnp.sum(jnp.where(slot_hits, route_weight[:, :, None], 0.0), axis=1)
    tok_float = tokens.astype(jnp.float32)
    square_sum = taken_together(jnp.sum(tok_float * tok_float, axis=1), TP)
    full_width = columns * lax.axis_size(TP)
    normed = (tok_float * lax.rsqrt(square_sum / full_width + epsilon)[:, None]).astype(
        jnp.bfloat16
    )
    padded = jnp.concatenate([normed, jnp.zeros((1, columns), jnp.bfloat16)], axis=0)
    outgoing = padded[lane_token].reshape(experts, capacity, columns)
    arrived = lax.all_to_all(outgoing, "fs", split_axis=0, concat_axis=0, tiled=True).reshape(
        -1, columns
    )
    gate_local = gate_new[0]
    up_local = up_new[0]
    piece_rows = lax.all_gather(arrived, TP, axis=1, tiled=True)
    gate_acc = jnp.dot(piece_rows, gate_local, preferred_element_type=jnp.float32)
    up_acc = jnp.dot(piece_rows, up_local, preferred_element_type=jnp.float32)
    hidden = (jax.nn.silu(gate_acc) * up_acc).astype(jnp.bfloat16)
    down_local = down_new[0]
    summed = scatter_axes(
        lax.dot_general(
            down_local, hidden, (((1,), (1,)), ((), ())), preferred_element_type=jnp.float32
        ).astype(jnp.bfloat16),
        TP,
        (1, 0),
        0,
    ).astype(jnp.float32)
    own_columns = summed.shape[0]
    outgoing_back = summed.astype(jnp.bfloat16).reshape(own_columns, fs_count, capacity)
    returned = lax.all_to_all(outgoing_back, "fs", split_axis=1, concat_axis=1, tiled=True).reshape(
        own_columns, experts * capacity
    )
    mixed = lax.dot_general(
        combine,
        returned.astype(jnp.float32),
        (((1,), (1,)), ((), ())),
        preferred_element_type=jnp.float32,
    )
    return (mixed.astype(jnp.bfloat16), gate_new, up_new, down_new)


def solution(mesh):
    split = Mesh(mesh.devices.reshape(mesh.shape["fs"], 16, 2), ("fs", "tp_0", "tp_1"))
    in_specs = (
        P("fs", TP),
        P("fs"),
        P(None, "fs", TP),
        P(None, "fs", TP),
        P(None, "fs", TP),
        P("fs", None),
        P("fs", None),
    )
    out_specs = (P("fs", TP), P("fs", None, TP), P("fs", None, TP), P("fs", None, TP))
    return jax.shard_map(body, mesh=split, in_specs=in_specs, out_specs=out_specs, check_vma=False)
```

profile of v0, /device:TPU:32, one launch (start us, length us, event | category | flops | bytes accessed | tf_op | source)
XLA Modules:
  0.0 259.3 jit_solution(12488290934281086768)
XLA Ops:
  7.2 0.8 fusion.12
  7.9 0.6 broadcast_in_dim.45
  8.6 15.4 %all-to-all-start.1 = ((f32[32,1,256]{2,1,0:T(1,128)}), f32[32,1,256]{2,1,0:T(1,128)S(1)}, u32[]{:S(2)}, u32[]{:S(2)}) async-start(f32[32,1,256]{2,1,0:T(1,128)} %broadcast_in_dim.45), calls=%async_computation.1 | async-start | bytes 65536 | tf_op jit(solution)/shard_map/all_to_all | solution.py:26
  23.9 0.0 all-gather.2.cloned.1.call-start
  24.0 0.8 copy.71
  24.8 0.1 eq.40
  25.0 1.2 reduce-window.6
  26.2 0.2 slice_reduce_fusion
  26.5 0.1 copy.74
  26.5 0.1 broadcast.115
  26.6 0.1 fusion.14
  26.7 0.1 reshape.194
  26.9 0.1 copy.75
  26.9 0.7 multiply_add_fusion
  27.6 0.3 select_reduce_fusion
  28.0 7.7 %all-to-all-done.1 = f32[32,1,256]{2,1,0:T(1,128)S(1)} async-done(((f32[32,1,256]{2,1,0:T(1,128)}), f32[32,1,256]{2,1,0:T(1,128)S(1)}, u32[]{:S(2)}, u32[]{:S(2)}) %all-to-all-start.1) | async-done | bytes 32800 | tf_op jit(solution)/shard_map/all_to_all | solution.py:26
  35.7 0.1 reduce_sum.48
  35.8 0.8 fusion.13
  36.5 0.1 copy.84
  36.7 3.2 %gather_fusion = bf16[1024,64]{1,0:T(8,128)(2,1)S(1)} fusion(bf16[257,64]{1,0:T(8,128)(2,1)S(1)} %concatenate.7.clone, s32[1024]{0:T(1024)S(1)} %broadcast_clamp_fusion), kind=kCustom, calls=%fused_computation | custom fusion | bytes 266240 | tf_op jit(solution)/shard_map/gather | solution.py:89
  39.9 0.0 copy-start.4
  39.9 0.0 copy-start.5
  39.9 0.0 copy-start.7
  39.9 0.2 reshape.209
  40.2 15.1 %all_to_all.28 = bf16[16,2,2048]{2,1,0:T(2,128)(2,1)} all-to-all(bf16[16,2,2048]{2,1,0:T(2,128)(2,1)S(1)} %reshape.209), channel_id=1, replica_groups=mesh['fs'=16,'tp_0'=16,'tp_1'=2] {'fs'}, dimensions={0} | all-to-all | bytes 262144 | tf_op jit(solution)/shard_map/all_to_all | solution.py:90
  55.2 1.1 reshape.210
  56.4 0.8 copy.82
  57.1 0.0 all-gather.2.cloned.1.call-update
  57.2 0.0 reduce-scatter.3.cloned.1.call-start
  57.2 0.0 copy-done.3
  57.2 0.1 convert_element_type.41
  57.3 0.0 copy-done.4
  57.3 0.0 copy-done.5
  57.3 0.3 multiply_convert_fusion.1
  57.7 0.2 pad_maximum_fusion
  57.9 24.3 %all_to_all.29 = bf16[16,128,384]{2,1,0:T(8,128)(2,1)S(1)} all-to-all(bf16[16,128,384]{2,1,0:T(8,128)(2,1)S(1)} %pad_maximum_fusion), channel_id=1, replica_groups=mesh['fs'=16,'tp_0'=16,'tp_1'=2] {'fs'}, dimensions={0} | all-to-all | bytes 3145728 | tf_op jit(solution)/shard_map/all_to_all | solution.py:14
  82.3 0.3 fusion.16
  82.6 0.0 copy-start
  82.6 0.0 copy-start.1
  82.6 0.0 copy-start.2
  82.6 37.4 %all-gather.2.cloned.1.call-done = bf16[1024,2048]{0,1:T(8,128)(2,1)} async-done(((bf16[1024,64]{0,1:T(8,128)(2,1)}), bf16[1024,2048]{0,1:T(8,128)(2,1)}) %all-gather.2.cloned.1.call-update) | async-done | bytes 4194320 | tf_op jit(solution)/shard_map/all_gather | solution.py:95
  120.0 3.5 %fusion.3 = f32[1024,128]{1,0:T(8,128)S(1)} fusion(bf16[1024,2048]{0,1:T(8,128)(2,1)} %all-gather.2.cloned.1.call-done, bf16[1,2048,128]{2,1,0:T(8,128)(2,1)S(1)} %get-tuple-element.4), kind=kOutput, calls=%fused_computation.12 | convolution fusion | flops 536870912 | bytes 5242880 | tf_op jit(solution)/shard_map/dot_general | solution.py:96
  123.5 0.0 copy-done
  123.5 0.0 copy-done.1
  123.5 0.0 copy-done.2
  123.5 8.6 %convolution_convert_fusion = bf16[2048,1024]{1,0:T(8,128)(2,1)} fusion(bf16[1024,2048]{0,1:T(8,128)(2,1)} %all-gather.2.cloned.1.call-done, bf16[1,2048,128]{2,1,0:T(8,128)(2,1)S(1)} %get-tuple-element.5, bf16[1,2048,128]{2,1,0:T(8,128)(2,1)S(1)} %get-tuple-element.6, f32[1024,128]{1,0:T(8,128)S(1)} %fusion.3), kind=kOutput, calls=%fused_computation.1 | convolution fusion | flops 1076625408 | bytes 9961472 | tf_op jit(solution)/shard_map/dot_general | solution.py:101
  132.1 4.8 %copy.79 = bf16[16,2,64,1024]{3,2,0,1:T(8,128)(2,1)} copy(bf16[16,2,64,1024]{3,2,1,0:T(8,128)(2,1)} %bitcast.42) | data formatting | bytes 8388608 | tf_op jit(solution)/shard_map/reshape;reshape | solution.py:35
  136.9 0.0 reduce-scatter.3.cloned.1.call-update
  137.0 0.0 copy-start.6
  137.0 0.0 reduce-scatter.5.cloned.1.call-start
  137.0 19.7 %reduce-scatter.3.cloned.1.call-done = bf16[16,64,1024]{2,1,0:T(8,128)(2,1)} async-done(((bf16[32,64,1024]{2,1,0:T(8,128)(2,1)}), bf16[16,64,1024]{2,1,0:T(8,128)(2,1)}) %reduce-scatter.3.cloned.1.call-update) | async-done | bytes 2097168 | tf_op jit(solution)/shard_map/reduce_scatter | solution.py:39
  156.7 0.0 reduce-scatter.5.cloned.1.call-update
  156.7 77.7 %reduce-scatter.5.cloned.1.call-done = bf16[1,64,1024]{2,1,0:T(8,128)(2,1)} async-done(((bf16[16,64,1024]{2,1,0:T(8,128)(2,1)}), bf16[1,64,1024]{2,1,0:T(8,128)(2,1)}) %reduce-scatter.5.cloned.1.call-update) | async-done | bytes 131088 | tf_op jit(solution)/shard_map/reduce_scatter | solution.py:39
  234.4 1.1 reshape.198
  235.5 0.1 copy.86
  235.6 0.9 reshape.211
  236.5 6.8 %all-to-all-start.3 = ((bf16[16,2,2048]{2,1,0:T(2,128)(2,1)}), bf16[16,2,2048]{2,1,0:T(2,128)(2,1)S(1)}, u32[]{:S(2)}, u32[]{:S(2)}) async-start(bf16[16,2,2048]{2,1,0:T(2,128)(2,1)} %reshape.211), calls=%async_computation.5 | async-start | bytes 262144 | tf_op jit(solution)/shard_map/all_to_all | solution.py:110
  243.3 0.0 copy-done.6
  243.3 0.3 select_reduce_fusion.1
  243.6 7.7 %all-to-all-done.3 = bf16[16,2,2048]{2,1,0:T(2,128)(2,1)S(1)} async-done(((bf16[16,2,2048]{2,1,0:T(2,128)(2,1)}), bf16[16,2,2048]{2,1,0:T(2,128)(2,1)S(1)}, u32[]{:S(2)}, u32[]{:S(2)}) %all-to-all-start.3) | async-done | bytes 131104 | tf_op jit(solution)/shard_map/all_to_all | solution.py:110
  251.3 0.2 reshape.212
  251.5 0.2 copy.81
  251.7 0.2 reshape.199
  251.9 0.9 fusion.17
  (13 shorter events, 0.1 us)
Async XLA Ops:
  8.6 27.1 %all-to-all-start.1 = ((f32[32,1,256]{2,1,0:T(1,128)}), f32[32,1,256]{2,1,0:T(1,128)S(1)}, u32[]{:S(2)}, u32[]{:S(2)}) async-start(f32[32,1,256]{2,1,0:T(1,128)} %broadcast_in_dim.45), calls=%async_computation.1 | async-start | bytes 65536 | tf_op jit(solution)/shard_map/all_to_all | solution.py:26
  23.9 96.1 %all-gather.2.cloned.1.call-start = ((), (), s32[]{:S(2)}) async-start(), calls=%async_computation.6 | async-start | bytes 4325376 | tf_op jit(solution)/shard_map/all_gather | solution.py:95
  36.5 20.7 %copy-start.3 = (f32[16,128,128]{2,1,0:T(8,128)S(1)}, f32[16,128,128]{2,1,0:T(8,128)}, u32[]{:S(2)}) copy-start(f32[16,128,128]{2,1,0:T(8,128)} %param.11) | copy-start | bytes 3145732
  39.9 17.4 %copy-start.4 = (f32[16,128,128]{2,1,0:T(8,128)S(1)}, f32[16,128,128]{2,1,0:T(8,128)}, u32[]{:S(2)}) copy-start(f32[16,128,128]{2,1,0:T(8,128)} %param.9) | copy-start | bytes 3145732
  39.9 17.4 %copy-start.5 = (f32[16,128,128]{2,1,0:T(8,128)S(1)}, f32[16,128,128]{2,1,0:T(8,128)}, u32[]{:S(2)}) copy-start(f32[16,128,128]{2,1,0:T(8,128)} %param.10) | copy-start | bytes 3145732
  39.9 17.4 %copy-start.7 = (f32[128]{0:T(128)S(1)}, f32[128]{0:T(128)}, u32[]{:S(2)}) copy-start(f32[128]{0:T(128)} %param.8) | copy-start | bytes 1540
  57.2 99.5 %reduce-scatter.3.cloned.1.call-start = ((), (), s32[]{:S(2)}) async-start(), calls=%async_computation.7 | async-start | bytes 6291456 | tf_op jit(solution)/shard_map/reduce_scatter | solution.py:39
  82.6 40.9 %copy-start = (bf16[1,2048,128]{2,1,0:T(8,128)(2,1)}, bf16[1,2048,128]{2,1,0:T(8,128)(2,1)S(1)}, u32[]{:S(2)}) copy-start(bf16[1,2048,128]{2,1,0:T(8,128)(2,1)S(1)} %get-tuple-element.4) | copy-start | bytes 1572868
  82.6 40.9 %copy-start.1 = (bf16[1,2048,128]{2,1,0:T(8,128)(2,1)}, bf16[1,2048,128]{2,1,0:T(8,128)(2,1)S(1)}, u32[]{:S(2)}) copy-start(bf16[1,2048,128]{2,1,0:T(8,128)(2,1)S(1)} %get-tuple-element.5) | copy-start | bytes 1572868
  82.6 40.9 %copy-start.2 = (bf16[1,2048,128]{2,1,0:T(8,128)(2,1)}, bf16[1,2048,128]{2,1,0:T(8,128)(2,1)S(1)}, u32[]{:S(2)}) copy-start(bf16[1,2048,128]{2,1,0:T(8,128)(2,1)S(1)} %get-tuple-element.6) | copy-start | bytes 1572868
  137.0 106.3 %copy-start.6 = (f32[256,2]{0,1:T(2,128)S(1)}, f32[256,2]{0,1:T(2,128)}, u32[]{:S(2)}) copy-start(f32[256,2]{0,1:T(2,128)} %param.13) | copy-start | bytes 6148
  137.0 97.4 %reduce-scatter.5.cloned.1.call-start = ((), (), s32[]{:S(2)}) async-start(), calls=%async_computation.8 | async-start | bytes 2228224 | tf_op jit(solution)/shard_map/reduce_scatter | solution.py:39
  236.5 14.8 %all-to-all-start.3 = ((bf16[16,2,2048]{2,1,0:T(2,128)(2,1)}), bf16[16,2,2048]{2,1,0:T(2,128)(2,1)S(1)}, u32[]{:S(2)}, u32[]{:S(2)}) async-start(bf16[16,2,2048]{2,1,0:T(2,128)(2,1)} %reshape.211), calls=%async_computation.5 | async-start | bytes 262144 | tf_op jit(solution)/shard_map/all_to_all | solution.py:110
Sparse Core Ops, SparseCore 0:
  57.3 62.7 all-gather.1
  137.1 19.5 reduce-scatter.2
  159.5 74.8 reduce-scatter.4
where the time goes:
time: 260 us; the launch traced here: 259 us
  waiting for transfers between devices  150 us (58%)
  blocking collectives  39.4 us (15%)
  starting transfers between devices  22.3 us (9%)
  local copies, waits for them, and re-layouts  15.5 us (6%)
  between operations  14.1 us (5%)
  matrix products  13 us (5%)
  other arithmetic  4.87 us (2%)
    reduce_scatter x2, waiting for transfers between devices, reduced_to_own(): pieces = lax.psum_scatter(pieces, axes[k], scatter_dimension=0, tiled=True)  97.4 us
    all_gather x1, waiting for transfers between devices, body(): piece_rows = lax.all_gather(arrived, TP, axis=1, tiled=True)  37.4 us
    all_to_all x1, blocking collectives, sent_together(): lax.all_to_all(both, axis, split_axis=split_dim, concat_axis=concat_dim,...  24.3 us
    all_to_all x1, starting transfers between devices, sent_to_all(): lax.all_to_all(jnp.broadcast_to(x[None], (peers, *x.shape)), axis, 0, 0,...  15.4 us
    all_to_all x1, blocking collectives, body(): lax.all_to_all(outgoing, 'fs', split_axis=0, concat_axis=0, tiled=True)  15.1 us
    dot_general x1, matrix products, body(): lax.dot_general(down_local, hidden, (((1,), (1,)), ((), ())), preferred_e...  8.59 us
    all_to_all x1, waiting for transfers between devices, sent_to_all(): lax.all_to_all(jnp.broadcast_to(x[None], (peers, *x.shape)), axis, 0, 0,...  7.74 us
    all_to_all x1, waiting for transfers between devices, body(): lax.all_to_all(outgoing_back, 'fs', split_axis=1, concat_axis=1, tiled=True)  7.69 us
  transfers between devices with their start and end apart: 5, of which 5 were waited for; matrix products, arithmetic and copies ran while one was open for 2% of the time, Pallas kernels for 0%

commit v1 on v0

--- a/solution.py
+++ b/solution.py
@@ -6,6 +6,12 @@
 
 TP = ("tp_0", "tp_1")
 epsilon = 1e-05
+
+
+def scan_modes(original):
+    return jnp.concatenate(
+        jax.lax.all_to_all(jnp.stack(jax.lax.axis_size(TP) * [original]), TP, 0, 0), axis=1
+    )
 
 
 def sent_together(arrays, axis, split_dim, concat_dim, along):
@@ -92,7 +98,7 @@
     )
     gate_local = gate_new[0]
     up_local = up_new[0]
-    piece_rows = lax.all_gather(arrived, TP, axis=1, tiled=True)
+    piece_rows = scan_modes(arrived)
     gate_acc = jnp.dot(piece_rows, gate_local, preferred_element_type=jnp.float32)
     up_acc = jnp.dot(piece_rows, up_local, preferred_element_type=jnp.float32)
     hidden = (jax.nn.silu(gate_acc) * up_acc).astype(jnp.bfloat16)

time: 260 us -> 413 us (1.59)
  the two profiles are of different devices: /device:TPU:32 before, /device:TPU:2 now
where the time goes in v1:
time: 413 us
  waiting for transfers between devices  318 us (77%)
  starting transfers between devices  42.1 us (10%)
  local copies, waits for them, and re-layouts  17.1 us (4%)
  between operations  14.3 us (3%)
  matrix products  13 us (3%)
  other arithmetic  7.81 us (2%)
    all_to_all x1, waiting for transfers between devices, scan_modes(): jax.lax.all_to_all(jnp.stack(jax.lax.axis_size(TP) * [original]), TP, 0, 0)  183 us
    reduce_scatter x2, waiting for transfers between devices, reduced_to_own(): pieces = lax.psum_scatter(pieces, axes[k], scatter_dimension=0, tiled=True)  97.8 us
    all_to_all x1, waiting for transfers between devices, sent_together(): lax.all_to_all(both, axis, split_axis=split_dim, concat_axis=concat_dim,...  19.6 us
    all_to_all x1, starting transfers between devices, sent_to_all(): lax.all_to_all(jnp.broadcast_to(x[None], (peers, *x.shape)), axis, 0, 0,...  15.5 us
    dot_general x1, matrix products, body(): lax.dot_general(down_local, hidden, (((1,), (1,)), ((), ())), preferred_e...  8.59 us
  transfers between devices with their start and end apart: 7, of which 7 were waited for; matrix products, arithmetic and copies ran while one was open for 2% of the time, Pallas kernels for 0%

profile of v1, /device:TPU:2, one launch (start us, length us, event | category | flops | bytes accessed | tf_op | source)
XLA Modules:
  0.0 412.5 jit_solution(13219871085599472936)
XLA Ops:
  7.2 0.0 copy-start.4
  7.2 0.0 copy-start.3
  7.2 0.9 fusion.12
  8.1 0.6 broadcast_in_dim.45
  8.7 15.5 %all-to-all-start.1 = ((f32[32,1,256]{2,1,0:T(1,128)}), f32[32,1,256]{2,1,0:T(1,128)S(1)}, u32[]{:S(2)}, u32[]{:S(2)}) async-start(f32[32,1,256]{2,1,0:T(1,128)} %broadcast_in_dim.45), calls=%async_computation.1 | async-start | bytes 65536 | tf_op jit(solution)/shard_map/all_to_all | solution.py:32
  24.2 0.8 copy.72
  25.0 0.1 eq.40
  25.2 1.2 reduce-window.6
  26.3 0.2 slice_reduce_fusion
  26.6 0.1 copy.75
  26.7 0.1 broadcast.116
  26.8 0.1 fusion.14
  26.9 0.1 reshape.199
  27.0 0.1 copy.76
  27.1 0.7 multiply_add_fusion
  27.8 0.3 select_reduce_fusion
  28.1 1.3 convert_element_type.41
  29.5 0.0 copy-done.3
  29.5 1.6 multiply_convert_fusion.1
  31.1 6.1 %all-to-all-done.1 = f32[32,1,256]{2,1,0:T(1,128)S(1)} async-done(((f32[32,1,256]{2,1,0:T(1,128)}), f32[32,1,256]{2,1,0:T(1,128)S(1)}, u32[]{:S(2)}, u32[]{:S(2)}) %all-to-all-start.1) | async-done | bytes 32800 | tf_op jit(solution)/shard_map/all_to_all | solution.py:32
  37.2 0.1 reduce_sum.48
  37.2 0.0 copy-done.4
  37.2 0.1 copy.84
  37.4 3.2 gather_fusion
  40.6 0.9 reshape.215
  41.5 7.5 %all-to-all-start.2 = ((bf16[16,2,2048]{2,1,0:T(2,128)(2,1)}), bf16[16,2,2048]{2,1,0:T(2,128)(2,1)S(1)}, u32[]{:S(2)}, u32[]{:S(2)}) async-start(bf16[16,2,2048]{2,1,0:T(2,128)(2,1)} %reshape.215), calls=%async_computation.2 | async-start | bytes 262144 | tf_op jit(solution)/shard_map/all_to_all | solution.py:96
  49.0 1.4 pad_maximum_fusion
  50.4 5.2 %all-to-all-done.2 = bf16[16,2,2048]{2,1,0:T(2,128)(2,1)S(1)} async-done(((bf16[16,2,2048]{2,1,0:T(2,128)(2,1)}), bf16[16,2,2048]{2,1,0:T(2,128)(2,1)S(1)}, u32[]{:S(2)}, u32[]{:S(2)}) %all-to-all-start.2) | async-done | bytes 131104 | tf_op jit(solution)/shard_map/all_to_all | solution.py:96
  55.6 5.0 %all-to-all-start = ((bf16[16,128,384]{2,1,0:T(8,128)(2,1)}), bf16[16,128,384]{2,1,0:T(8,128)(2,1)S(1)}, u32[]{:S(2)}, u32[]{:S(2)}) async-start(bf16[16,128,384]{2,1,0:T(8,128)(2,1)} %pad_maximum_fusion), calls=%async_computation | async-start | bytes 3145728 | tf_op jit(solution)/shard_map/all_to_all | solution.py:20
  60.6 0.2 reshape.216
  60.8 0.1 copy.79
  60.9 19.6 %all-to-all-done = bf16[16,128,384]{2,1,0:T(8,128)(2,1)S(1)} async-done(((bf16[16,128,384]{2,1,0:T(8,128)(2,1)}), bf16[16,128,384]{2,1,0:T(8,128)(2,1)S(1)}, u32[]{:S(2)}, u32[]{:S(2)}) %all-to-all-start) | async-done | bytes 1572896 | tf_op jit(solution)/shard_map/all_to_all | solution.py:20
  80.5 2.5 stack.3
  83.0 7.0 %all-to-all-start.3 = ((bf16[32,1024,64]{1,2,0:T(8,128)(2,1)}), bf16[32,1024,64]{1,2,0:T(8,128)(2,1)}, u32[]{:S(2)}, u32[]{:S(2)}) async-start(bf16[32,1024,64]{1,2,0:T(8,128)(2,1)} %stack.3), calls=%async_computation.3 | async-start | bytes 8388608 | tf_op jit(solution)/shard_map/all_to_all | solution.py:13
  90.0 0.0 reduce-scatter.3.cloned.1.call-start
  90.1 0.3 fusion.16
  90.4 0.0 copy-start
  90.4 0.0 copy-start.1
  90.4 0.0 copy-start.2
  90.4 183.1 %all-to-all-done.3 = bf16[32,1024,64]{1,2,0:T(8,128)(2,1)} async-done(((bf16[32,1024,64]{1,2,0:T(8,128)(2,1)}), bf16[32,1024,64]{1,2,0:T(8,128)(2,1)}, u32[]{:S(2)}, u32[]{:S(2)}) %all-to-all-start.3) | async-done | bytes 4194336 | tf_op jit(solution)/shard_map/all_to_all | solution.py:13
  273.5 3.5 fusion.3
  277.0 8.6 %convolution_convert_fusion = bf16[2048,1024]{1,0:T(8,128)(2,1)} fusion(bf16[1024,2048]{0,1:T(8,128)(2,1)} %bitcast.13, bf16[1,2048,128]{2,1,0:T(8,128)(2,1)S(1)} %get-tuple-element.5, bf16[1,2048,128]{2,1,0:T(8,128)(2,1)S(1)} %get-tuple-element.6, f32[1024,128]{1,0:T(8,128)S(1)} %fusion.3), kind=kOutput, calls=%fused_computation.1 | convolution fusion | flops 1076625408 | bytes 9961472 | tf_op jit(solution)/shard_map/dot_general | solution.py:107
  285.6 0.0 copy-done
  285.6 0.0 copy-done.1
  285.6 0.0 copy-done.2
  285.6 4.8 %copy.80 = bf16[16,2,64,1024]{3,2,0,1:T(8,128)(2,1)} copy(bf16[16,2,64,1024]{3,2,1,0:T(8,128)(2,1)} %bitcast.45) | data formatting | bytes 8388608 | tf_op jit(solution)/shard_map/reshape;reshape | solution.py:41
  290.4 0.0 copy-start.5
  290.4 0.0 reduce-scatter.3.cloned.1.call-update
  290.4 0.0 reduce-scatter.5.cloned.1.call-start
  290.5 19.5 %reduce-scatter.3.cloned.1.call-done = bf16[16,64,1024]{2,1,0:T(8,128)(2,1)} async-done(((bf16[32,64,1024]{2,1,0:T(8,128)(2,1)}), bf16[16,64,1024]{2,1,0:T(8,128)(2,1)}) %reduce-scatter.3.cloned.1.call-update) | async-done | bytes 2097168 | tf_op jit(solution)/shard_map/reduce_scatter | solution.py:45
  310.0 0.0 reduce-scatter.5.cloned.1.call-update
  310.0 78.4 %reduce-scatter.5.cloned.1.call-done = bf16[1,64,1024]{2,1,0:T(8,128)(2,1)} async-done(((bf16[16,64,1024]{2,1,0:T(8,128)(2,1)}), bf16[1,64,1024]{2,1,0:T(8,128)(2,1)}) %reduce-scatter.5.cloned.1.call-update) | async-done | bytes 131088 | tf_op jit(solution)/shard_map/reduce_scatter | solution.py:45
  388.3 1.1 reshape.204
  389.5 0.1 copy.86
  389.5 0.9 reshape.217
  390.4 7.1 %all-to-all-start.4 = ((bf16[16,2,2048]{2,1,0:T(2,128)(2,1)}), bf16[16,2,2048]{2,1,0:T(2,128)(2,1)S(1)}, u32[]{:S(2)}, u32[]{:S(2)}) async-start(bf16[16,2,2048]{2,1,0:T(2,128)(2,1)} %reshape.217), calls=%async_computation.6 | async-start | bytes 262144 | tf_op jit(solution)/shard_map/all_to_all | solution.py:116
  397.5 0.0 copy-done.5
  397.6 0.3 select_reduce_fusion.1
  397.8 6.3 %all-to-all-done.4 = bf16[16,2,2048]{2,1,0:T(2,128)(2,1)S(1)} async-done(((bf16[16,2,2048]{2,1,0:T(2,128)(2,1)}), bf16[16,2,2048]{2,1,0:T(2,128)(2,1)S(1)}, u32[]{:S(2)}, u32[]{:S(2)}) %all-to-all-start.4) | async-done | bytes 131104 | tf_op jit(solution)/shard_map/all_to_all | solution.py:116
  404.2 0.2 reshape.218
  404.4 0.2 copy.82
  404.6 0.2 reshape.205
  404.8 0.9 fusion.17
  (12 shorter events, 0.2 us)
Async XLA Ops:
  7.2 30.1 %copy-start.4 = (bf16[256,64]{0,1:T(8,128)(2,1)S(1)}, bf16[256,64]{0,1:T(8,128)(2,1)}, u32[]{:S(2)}) copy-start(bf16[256,64]{0,1:T(8,128)(2,1)} %param.7) | copy-start | bytes 98308
  7.2 22.3 %copy-start.3 = (f32[16,128,128]{2,1,0:T(8,128)S(1)}, f32[16,128,128]{2,1,0:T(8,128)}, u32[]{:S(2)}) copy-start(f32[16,128,128]{2,1,0:T(8,128)} %param.9) | copy-start | bytes 3145732
  8.7 28.5 %all-to-all-start.1 = ((f32[32,1,256]{2,1,0:T(1,128)}), f32[32,1,256]{2,1,0:T(1,128)S(1)}, u32[]{:S(2)}, u32[]{:S(2)}) async-start(f32[32,1,256]{2,1,0:T(1,128)} %broadcast_in_dim.45), calls=%async_computation.1 | async-start | bytes 65536 | tf_op jit(solution)/shard_map/all_to_all | solution.py:32
  41.5 14.1 %all-to-all-start.2 = ((bf16[16,2,2048]{2,1,0:T(2,128)(2,1)}), bf16[16,2,2048]{2,1,0:T(2,128)(2,1)S(1)}, u32[]{:S(2)}, u32[]{:S(2)}) async-start(bf16[16,2,2048]{2,1,0:T(2,128)(2,1)} %reshape.215), calls=%async_computation.2 | async-start | bytes 262144 | tf_op jit(solution)/shard_map/all_to_all | solution.py:96
  55.6 24.9 %all-to-all-start = ((bf16[16,128,384]{2,1,0:T(8,128)(2,1)}), bf16[16,128,384]{2,1,0:T(8,128)(2,1)S(1)}, u32[]{:S(2)}, u32[]{:S(2)}) async-start(bf16[16,128,384]{2,1,0:T(8,128)(2,1)} %pad_maximum_fusion), calls=%async_computation | async-start | bytes 3145728 | tf_op jit(solution)/shard_map/all_to_all | solution.py:20
  83.0 190.5 %all-to-all-start.3 = ((bf16[32,1024,64]{1,2,0:T(8,128)(2,1)}), bf16[32,1024,64]{1,2,0:T(8,128)(2,1)}, u32[]{:S(2)}, u32[]{:S(2)}) async-start(bf16[32,1024,64]{1,2,0:T(8,128)(2,1)} %stack.3), calls=%async_computation.3 | async-start | bytes 8388608 | tf_op jit(solution)/shard_map/all_to_all | solution.py:13
  90.0 219.9 %reduce-scatter.3.cloned.1.call-start = ((), (), s32[]{:S(2)}) async-start(), calls=%async_computation.7 | async-start | bytes 6291456 | tf_op jit(solution)/shard_map/reduce_scatter | solution.py:45
  90.4 195.2 %copy-start = (bf16[1,2048,128]{2,1,0:T(8,128)(2,1)}, bf16[1,2048,128]{2,1,0:T(8,128)(2,1)S(1)}, u32[]{:S(2)}) copy-start(bf16[1,2048,128]{2,1,0:T(8,128)(2,1)S(1)} %get-tuple-element.4) | copy-start | bytes 1572868
  90.4 195.2 %copy-start.1 = (bf16[1,2048,128]{2,1,0:T(8,128)(2,1)}, bf16[1,2048,128]{2,1,0:T(8,128)(2,1)S(1)}, u32[]{:S(2)}) copy-start(bf16[1,2048,128]{2,1,0:T(8,128)(2,1)S(1)} %get-tuple-element.5) | copy-start | bytes 1572868
  90.4 195.2 %copy-start.2 = (bf16[1,2048,128]{2,1,0:T(8,128)(2,1)}, bf16[1,2048,128]{2,1,0:T(8,128)(2,1)S(1)}, u32[]{:S(2)}) copy-start(bf16[1,2048,128]{2,1,0:T(8,128)(2,1)S(1)} %get-tuple-element.6) | copy-start | bytes 1572868
  290.4 107.1 %copy-start.5 = (f32[256,2]{0,1:T(2,128)S(1)}, f32[256,2]{0,1:T(2,128)}, u32[]{:S(2)}) copy-start(f32[256,2]{0,1:T(2,128)} %param.13) | copy-start | bytes 6148
  290.4 97.9 %reduce-scatter.5.cloned.1.call-start = ((), (), s32[]{:S(2)}) async-start(), calls=%async_computation.8 | async-start | bytes 2228224 | tf_op jit(solution)/shard_map/reduce_scatter | solution.py:45
  390.4 13.7 %all-to-all-start.4 = ((bf16[16,2,2048]{2,1,0:T(2,128)(2,1)}), bf16[16,2,2048]{2,1,0:T(2,128)(2,1)S(1)}, u32[]{:S(2)}, u32[]{:S(2)}) async-start(bf16[16,2,2048]{2,1,0:T(2,128)(2,1)} %reshape.217), calls=%async_computation.6 | async-start | bytes 262144 | tf_op jit(solution)/shard_map/all_to_all | solution.py:116
Sparse Core Ops, SparseCore 0:
  290.6 19.3 reduce-scatter.2
  312.8 75.5 reduce-scatter.4
